TPU v7x, 32 devices: a whole 2x2x4 slice. The times are simulated.
32 devices in a mesh: ep: 8 (over z, core), tp: 4 (over y, x).
Axes of the slice: x: 2, y: 2, z: 4, core: 2. Of those that a mesh axis runs over, the one named last changes fastest.
Arguments:
- query_input: bfloat16 [4096, 2048], P('ep', 'tp'), may hold values from -6 to 6
- key_input: bfloat16 [4096, 1024], P('ep', 'tp'), may hold values from -6 to 6
- value_input: bfloat16 [4096, 1024], P('ep', 'tp'), may hold values from -64 to 64
- query_gain: float32 [64], replicated, may hold values from 0.5 to 6
- key_gain: float32 [64], replicated, may hold values from 0.5 to 6
- mixer_out: bfloat16 [2048, 4096], P(None, 'tp'), may hold values from -0.125 to 0.125
- moe_input: bfloat16 [2048, 4096], P('ep'), may hold values from -6 to 6
- moe_gain: float32 [4096], replicated, may hold values from 0.1 to 1.9
- routes: int32 [2048, 2], P('ep'), may hold values from 0 to 7, all different within a row; in each aligned block of 256 rows (0 to 255, 256 to 511, ...) at most 96 rows name the same one
- route_weight: float32 [2048, 2], P('ep'), may hold values from 0.1 to 1
- expert_gate: bfloat16 [8, 4096, 1024], P('ep', None, 'tp'), may hold values from -0.09375 to 0.09375
- expert_up: bfloat16 [8, 4096, 1024], P('ep', None, 'tp'), may hold values from -0.09375 to 0.09375
- expert_down: bfloat16 [8, 1024, 4096], P('ep', None, 'tp'), may hold values from -0.1875 to 0.1875
Outputs:
- attn_mixed: bfloat16 [4096, 4096], P('ep', 'tp')
- moe_out: bfloat16 [2048, 4096], P('ep', 'tp')
Inputs may be any that keep to these rules, and one draw needn't show every extreme that they name: `routes`: each row names 2 different experts. In the rows of one index of ep (aligned blocks of 256 rows) no expert is named by more than 96 rows, and in every draw some block has an expert named by exactly 96 rows.
All inputs are finite; a program needn't handle non-finite values.
Results may differ from a plain program's by a relative error of at most 0.0095.
The roundings to bfloat16 on the way count: a program that leaves them out, or rounds other values in their place, can miss the bound.
Values may be sent and summed in bfloat16 or wider, within the bound.
A program may use at most 64 MiB of HBM per device.

v0:
```python
import functools
import math

import jax
import jax.numpy as jnp
from jax import lax
from jax.experimental import pallas as pl
from jax.experimental.pallas import tpu as pltpu
from jax.sharding import PartitionSpec as P

GRID_W = 64
CORES = 2

epsilon = 1e-06
base_theta = 10000.0


def rope_tables(positions, head_width):
    quarter = head_width // 4
    inverse = base_theta ** (-jnp.arange(quarter, dtype=jnp.float32) / quarter)
    grid_row = (positions // GRID_W).astype(jnp.float32)
    grid_col = (positions % GRID_W).astype(jnp.float32)
    angles = jnp.concatenate(
        [grid_row[:, None] * inverse[None, :], grid_col[:, None] * inverse[None, :]], axis=1
    )
    return (jnp.cos(angles), jnp.sin(angles))


def norm_rotate(columns, gain, cosine, sine, head_width):
    width = columns.shape[1]
    heads = width // head_width
    lane = jnp.arange(width)
    same_head = (lane[:, None] // head_width == lane[None, :] // head_width).astype(jnp.float32)
    half = head_width // 2
    within = lane % head_width
    partner = jnp.where(within < half, lane + half, lane - half)
    swap = (lane[:, None] == partner[None, :]).astype(jnp.bfloat16)
    values = columns.astype(jnp.float32)
    mean = (
        jnp.dot(values * values, same_head, precision=lax.Precision.HIGHEST) / head_width
    )
    scale = lax.rsqrt(mean + epsilon)
    swapped = jnp.dot(columns, swap, preferred_element_type=jnp.float32)
    gain_here = jnp.tile(gain, heads)[None, :]
    gain_swapped = jnp.tile(jnp.roll(gain, half), heads)[None, :]
    cos_here = jnp.tile(cosine, (1, 2 * heads))
    sin_here = jnp.tile(jnp.concatenate([-sine, sine], axis=1), (1, heads))
    return (
        values * scale * gain_here * cos_here + swapped * scale * gain_swapped * sin_here
    ).astype(jnp.bfloat16)


def kernel(
    dims,
    q_ref,
    kv_ref,
    disp_ref,
    pick_ref,
    share_ref,
    gate_hbm,
    up_hbm,
    down_hbm,
    mixer_hbm,
    attn_ref,
    moe_ref,
    kv_all,
    incoming,
    hid,
    eo,
    ret,
    att_all,
    gate_w,
    up_w,
    down_w,
    mixer_w,
    m_ref,
    l_ref,
    acc_ref,
    w_sem,
    loc_sem,
    d_send,
    d_recv,
    kv_send,
    kv_recv,
    f_send,
    g_send,
    g_recv,
    h_send,
    h_recv,
    r_send,
    r_recv,
    a_send,
    a_recv,
):
    n, T, head_width, hp = dims
    nz = n // CORES
    e = lax.axis_index("ep")
    t = lax.axis_index("tp")
    z = e // CORES
    c = e % CORES
    sibling = z * CORES + (1 - c)
    kh, rows, pw = q_ref.shape
    keys = kv_ref.shape[1]
    capp = disp_ref.shape[1]
    feat = disp_ref.shape[2]
    ffl = gate_w.shape[1]
    seq = attn_ref.shape[0]

    def offset(k):
        return ((k + 1) // 2) * (2 * (k % 2) - 1)

    def chip(k):
        return (z + offset(k) + 2 * nz) % nz

    def chip_to(k):
        return (z - offset(k) + 2 * nz) % nz

    def rdma(src, dst, ss, rs, axis, index):
        return pltpu.make_async_remote_copy(
            src_ref=src,
            dst_ref=dst,
            send_sem=ss,
            recv_sem=rs,
            device_id={axis: index},
            device_id_type=pl.DeviceIdType.MESH,
        )

    barrier = pltpu.get_barrier_semaphore()

    def greet(j, carry):
        pl.semaphore_signal(
            barrier, inc=1, device_id={"ep": (e + j) % n}, device_id_type=pl.DeviceIdType.MESH
        )
        return carry

    lax.fori_loop(1, n, greet, 0)
    for p in range(1, T):
        pl.semaphore_signal(
            barrier, inc=1, device_id={"tp": (t + p) % T}, device_id_type=pl.DeviceIdType.MESH
        )
    pl.semaphore_wait(barrier, n - 1 + T - 1)

    def d_copy(dest, origin):
        return rdma(
            disp_ref.at[dest], incoming.at[t, origin], d_send.at[dest], d_recv.at[origin], "ep", dest
        )

    def send_disp(k, carry):
        for cc in range(CORES):
            dest = chip_to(k) * CORES + cc

            @pl.when(dest != e)
            def _():
                d_copy(dest, e).start()

        return carry

    lax.fori_loop(0, nz, send_disp, 0)

    def kv_copy(dest, origin, ss):
        src = kv_ref if origin is None else kv_all.at[origin]
        slot = e if origin is None else origin
        return rdma(src, kv_all.at[slot], ss, kv_recv.at[slot], "ep", dest)

    kv_copy(sibling, None, f_send.at[z]).start()

    def send_kv(k, carry):
        zd = chip_to(k)
        kv_copy(zd * CORES + c, None, kv_send.at[zd]).start()
        return carry

    lax.fori_loop(1, nz, send_kv, 0)

    own_disp = pltpu.make_async_copy(disp_ref.at[e], incoming.at[t, e], loc_sem.at[0])
    own_disp.start()
    own_kv = pltpu.make_async_copy(kv_ref, kv_all.at[e], loc_sem.at[1])
    own_kv.start()
    loads = [
        pltpu.make_async_copy(gate_hbm, gate_w, w_sem.at[0]),
        pltpu.make_async_copy(up_hbm, up_w, w_sem.at[1]),
        pltpu.make_async_copy(down_hbm, down_w, w_sem.at[2]),
        pltpu.make_async_copy(mixer_hbm, mixer_w, w_sem.at[3]),
    ]
    for load in loads:
        load.start()
    own_disp.wait()
    own_kv.wait()

    def pair_at(k):
        return pl.ds(chip(k) * CORES, CORES)

    def g_copy(k, owner, peer):
        block = incoming.at[owner, pair_at(k)]
        return rdma(block, block, g_send.at[peer, k], g_recv.at[owner, k], "tp", peer)

    def h_copy(k, owner, peer):
        block = hid.at[owner, pair_at(k)]
        return rdma(block, block, h_send.at[peer, k], h_recv.at[owner, k], "tp", peer)

    def spread(k):
        for cc in range(CORES):
            origin = chip(k) * CORES + cc

            @pl.when(origin != e)
            def _():
                d_copy(origin, origin).wait_recv()

        for p in range(1, T):
            peer = (t + p) % T
            g_copy(k, t, peer).start()

    def attend_block(origin):
        def one_head(h, carry):
            lanes = pl.ds(pl.multiple_of((h * head_width) // pw * pw, pw), pw)
            key_block = kv_all[origin, 0, :, lanes] if kh > 1 else kv_all[origin, 0]
            value_block = kv_all[origin, 1, :, lanes] if kh > 1 else kv_all[origin, 1]
            step = math.gcd(rows, 256)
            for r in range(0, rows, step):
                at = slice(r, r + step)
                scores = lax.dot_general(
                    q_ref[h, at],
                    key_block,
                    (((1,), (1,)), ((), ())),
                    preferred_element_type=jnp.float32,
                )
                old = m_ref[h, at]
                new = jnp.maximum(old, jnp.max(scores, axis=1, keepdims=True))
                weights = jnp.exp(scores - new)
                factor = jnp.exp(old - new)
                m_ref[h, at] = new
                l_ref[h, at] = l_ref[h, at] * factor + jnp.sum(weights, axis=1, keepdims=True)
                acc_ref[h, at] = acc_ref[h, at] * factor + jnp.dot(
                    weights.astype(jnp.bfloat16), value_block, preferred_element_type=jnp.float32
                )
            return carry

        lax.fori_loop(0, kh, one_head, 0)

    def attend(k):
        zk = chip(k)
        mine = zk * CORES + c
        other = zk * CORES + (1 - c)

        @pl.when(k > 0)
        def _():
            kv_copy(mine, mine, kv_send.at[zk]).wait_recv()
            kv_copy(sibling, mine, f_send.at[zk]).start()

        attend_block(mine)
        kv_copy(sibling, other, f_send.at[zk]).wait_recv()
        attend_block(other)

    def first_half(k):
        for p in range(1, T):
            owner = (t + p) % T
            g_copy(k, owner, owner).wait_recv()
        gate = jnp.zeros((CORES * capp, ffl), jnp.float32)
        up = jnp.zeros((CORES * capp, ffl), jnp.float32)
        for s in range(T):
            piece = incoming[s, pair_at(k)].reshape(CORES * capp, feat)
            at = slice(s * feat, (s + 1) * feat)
            gate = gate + jnp.dot(piece, gate_w[at], preferred_element_type=jnp.float32)
            up = up + jnp.dot(piece, up_w[at], preferred_element_type=jnp.float32)
        hidden = (gate / (1.0 + jnp.exp(-gate)) * up).astype(jnp.bfloat16)
        hid[t, pair_at(k)] = hidden.reshape(CORES, capp, ffl)
        for p in range(1, T):
            peer = (t + p) % T
            h_copy(k, t, peer).start()

    def r_copy(dest, origin):
        return rdma(eo.at[dest], ret.at[origin], r_send.at[dest], r_recv.at[origin], "ep", dest)

    def second_half(k):
        for p in range(1, T):
            owner = (t + p) % T
            h_copy(k, owner, owner).wait_recv()
        total = jnp.zeros((CORES * capp, down_w.shape[1]), jnp.float32)
        for s in range(T):
            piece = hid[s, pair_at(k)].reshape(CORES * capp, ffl)
            total = total + jnp.dot(
                piece, down_w[s * ffl : (s + 1) * ffl], preferred_element_type=jnp.float32
            )
        eo[pair_at(k)] = total.astype(jnp.bfloat16).reshape(CORES, capp, down_w.shape[1])
        for cc in range(CORES):
            origin = chip(k) * CORES + cc

            @pl.when(origin != e)
            def _():
                r_copy(origin, e).start()

            @pl.when(origin == e)
            def _():
                ret[origin] = eo[origin]

    m_ref[...] = jnp.full(m_ref.shape, -jnp.inf, jnp.float32)
    l_ref[...] = jnp.zeros(l_ref.shape, jnp.float32)
    acc_ref[...] = jnp.zeros(acc_ref.shape, jnp.float32)

    ahead = min(2, nz)
    for k in range(ahead):
        spread(k)
    loads[0].wait()
    loads[1].wait()
    loads[2].wait()

    def step(k, carry):
        attend(k)
        first_half(k)

        @pl.when(k + ahead < nz)
        def _():
            spread(k + ahead)

        @pl.when(k >= 1)
        def _():
            second_half(k - 1)

        return carry

    lax.fori_loop(0, nz, step, 0)

    group = rows // seq
    for pair in range(kh * head_width // pw):
        heads = []
        for h in range(pair * (pw // head_width), (pair + 1) * (pw // head_width)):
            lane0 = (h * head_width) % pw
            done = acc_ref[h] / l_ref[h]
            for g in range(group):
                heads.append(done[g * seq : (g + 1) * seq, lane0 : lane0 + head_width])
        width = len(heads) * head_width
        att_all[t, :, pair * width : (pair + 1) * width] = jnp.concatenate(heads, axis=1).astype(
            jnp.bfloat16
        )

    def a_copy(owner, peer):
        block = att_all.at[owner]
        return rdma(block, block, a_send.at[peer], a_recv.at[owner], "tp", peer)

    for p in range(1, T):
        a_copy(t, (t + p) % T).start()
    second_half(nz - 1)
    loads[3].wait()
    for p in range(1, T):
        owner = (t + p) % T
        a_copy(owner, owner).wait_recv()
    aw = att_all.shape[2]
    out_cols = attn_ref.shape[1]
    half = math.gcd(out_cols, 256)

    def mix(i, carry):
        at = pl.ds(pl.multiple_of(i * half, half), half)
        total = jnp.zeros((seq, half), jnp.float32)
        for s in range(T):
            total = total + jnp.dot(
                att_all[s], mixer_w[s * aw : (s + 1) * aw, at], preferred_element_type=jnp.float32
            )
        attn_ref[:, at] = total.astype(jnp.bfloat16)
        return carry

    lax.fori_loop(0, out_cols // half, mix, 0)

    def wait_ret(j, carry):
        origin = (e + j) % n
        r_copy(origin, origin).wait_recv()
        return carry

    lax.fori_loop(1, n, wait_ret, 0)
    returned = ret[...].reshape(n * capp, ret.shape[2])
    tokens = moe_ref.shape[0]
    combined = jnp.zeros(moe_ref.shape, jnp.float32)
    for k in range(share_ref.shape[0]):
        combined = combined + share_ref[k] * jnp.dot(
            pick_ref[k], returned, preferred_element_type=jnp.float32
        )
    moe_ref[...] = combined.astype(jnp.bfloat16)

    def drain_ep(j, carry):
        dest = (e + j) % n
        d_copy(dest, e).wait_send()
        r_copy(dest, e).wait_send()
        return carry

    lax.fori_loop(1, n, drain_ep, 0)

    def drain_kv(k, carry):
        zd = chip_to(k)
        kv_copy(zd * CORES + c, None, kv_send.at[zd]).wait_send()
        return carry

    lax.fori_loop(1, nz, drain_kv, 0)

    def drain_tp(k, carry):
        kv_copy(sibling, e, f_send.at[k]).wait_send()
        for p in range(1, T):
            peer = (t + p) % T
            g_copy(k, t, peer).wait_send()
            h_copy(k, t, peer).wait_send()
        return carry

    lax.fori_loop(0, nz, drain_tp, 0)
    for p in range(1, T):
        a_copy(t, (t + p) % T).wait_send()


def on_device(
    n,
    T,
    query_input,
    key_input,
    value_input,
    query_gain,
    key_gain,
    mixer_out,
    moe_input,
    moe_gain,
    routes,
    route_weight,
    expert_gate,
    expert_up,
    expert_down,
):
    seq_dev = query_input.shape[0]
    head_width = query_gain.shape[0]
    heads_here = query_input.shape[1] // head_width
    kh = key_input.shape[1] // head_width
    kw = key_input.shape[1]
    group = heads_here // kh
    pw = min(128, kw)
    hp = pw // head_width
    positions = lax.axis_index("ep") * seq_dev + jnp.arange(seq_dev, dtype=jnp.int32)
    cosine, sine = rope_tables(positions, head_width)
    query_rot = norm_rotate(query_input, query_gain, cosine, sine, head_width)
    key_rot = norm_rotate(key_input, key_gain, cosine, sine, head_width)
    query_rot = query_rot * jnp.bfloat16(head_width ** (-0.5))
    by_head = []
    for h in range(kh):
        for g in range(group):
            col = (h * group + g) * head_width
            place = (h % hp) * head_width
            by_head.append(
                jnp.pad(
                    query_rot[:, col : col + head_width],
                    ((0, 0), (place, pw - head_width - place)),
                )
            )
    q_pad = jnp.stack(by_head).reshape(kh, group * seq_dev, pw)
    key_value = jnp.stack([key_rot, value_input])

    token_count, model_width = moe_input.shape
    top = routes.shape[1]
    local_experts = expert_gate.shape[0]
    assert local_experts == 1
    expert_count = local_experts * n
    capacity = 3 * token_count * top // (2 * expert_count)
    capp = -(-capacity // 16) * 16
    feat = model_width // T
    flat = routes.reshape(-1)
    pairs = token_count * top
    one_hot = flat[:, None] == jnp.arange(expert_count, dtype=jnp.int32)[None, :]
    order = jnp.arange(pairs, dtype=jnp.int32)
    before = (order[:, None] > order[None, :]).astype(jnp.bfloat16)
    earlier = jnp.dot(before, one_hot.astype(jnp.bfloat16), preferred_element_type=jnp.float32)
    slot = jnp.sum(jnp.where(one_hot, earlier, 0.0), axis=1).astype(jnp.int32)
    places = (flat * capp + slot).reshape(token_count, top)
    slots = jnp.arange(n * capp, dtype=jnp.int32)
    pick = (places.T[:, :, None] == slots[None, None, :]).astype(jnp.bfloat16)
    features = moe_input.astype(jnp.float32)
    inv = lax.rsqrt(jnp.mean(features * features, axis=-1, keepdims=True) + epsilon)
    start = lax.axis_index("tp") * feat
    own = lax.dynamic_slice_in_dim(moe_input, start, feat, 1).astype(jnp.float32)
    normed = (own * inv * lax.dynamic_slice_in_dim(moe_gain, start, feat, 0)).astype(jnp.bfloat16)
    disp = lax.dot_general(
        jnp.sum(pick, axis=0),
        normed,
        (((0,), (0,)), ((), ())),
        preferred_element_type=jnp.float32,
    ).astype(jnp.bfloat16)
    disp = disp.reshape(n, capp, feat)
    shares = route_weight / jnp.sum(route_weight, axis=-1, keepdims=True)
    shares = shares.T[:, :, None]

    gate = expert_gate[0]
    up = expert_up[0]
    down = expert_down[0]
    ffl = gate.shape[1]
    cols = down.shape[1]
    nz = n // CORES
    aw = heads_here * head_width
    out_cols = mixer_out.shape[1]
    bf = jnp.bfloat16
    dma = pltpu.SemaphoreType.DMA
    vmem = pl.BlockSpec(memory_space=pltpu.VMEM)
    hbm = pl.BlockSpec(memory_space=pl.ANY)
    return pl.pallas_call(
        functools.partial(kernel, (n, T, head_width, hp)),
        out_shape=(
            jax.ShapeDtypeStruct((seq_dev, out_cols), bf),
            jax.ShapeDtypeStruct((token_count, cols), bf),
        ),
        in_specs=[vmem] * 5 + [hbm] * 4,
        out_specs=(vmem, vmem),
        scratch_shapes=[
            pltpu.VMEM((n, 2, seq_dev, kw), bf),
            pltpu.VMEM((T, n, capp, feat), bf),
            pltpu.VMEM((T, n, capp, ffl), bf),
            pltpu.VMEM((n, capp, cols), bf),
            pltpu.VMEM((n, capp, cols), bf),
            pltpu.VMEM((T, seq_dev, aw), bf),
            pltpu.VMEM(gate.shape, bf),
            pltpu.VMEM(up.shape, bf),
            pltpu.VMEM(down.shape, bf),
            pltpu.VMEM(mixer_out.shape, bf),
            pltpu.VMEM((kh, group * seq_dev, 1), jnp.float32),
            pltpu.VMEM((kh, group * seq_dev, 1), jnp.float32),
            pltpu.VMEM((kh, group * seq_dev, pw), jnp.float32),
            dma((4,)),
            dma((2,)),
            dma((n,)),
            dma((n,)),
            dma((nz,)),
            dma((n,)),
            dma((nz,)),
            dma((T, nz)),
            dma((T, nz)),
            dma((T, nz)),
            dma((T, nz)),
            dma((n,)),
            dma((n,)),
            dma((T,)),
            dma((T,)),
        ],
        compiler_params=pltpu.CompilerParams(
            collective_id=0, has_side_effects=True, vmem_limit_bytes=63 * 1024 * 1024
        ),
    )(q_pad, key_value, disp, pick, shares, gate, up, down, mixer_out)


def solution(mesh):
    placed = (
        P("ep", "tp"),
        P("ep", "tp"),
        P("ep", "tp"),
        P(),
        P(),
        P(None, "tp"),
        P("ep", None),
        P(),
        P("ep", None),
        P("ep", None),
        P("ep", None, "tp"),
        P("ep", None, "tp"),
        P("ep", None, "tp"),
    )
    return jax.shard_map(
        functools.partial(on_device, mesh.shape["ep"], mesh.shape["tp"]),
        mesh=mesh,
        in_specs=placed,
        out_specs=(P("ep", "tp"), P("ep", "tp")),
        check_vma=False,
    )
```

profile of v0, /device:TPU:12, one launch (start us, length us, event | category | flops | bytes accessed | tf_op | source)
XLA Modules:
  0.0 177.8 jit_solution(1153714500054812108)
XLA Ops:
  0.6 0.0 copy-start.5
  0.7 0.0 copy-start.2
  0.7 0.0 copy-start
  0.7 2.2 %multiply_reduce_fusion = f32[256]{0:T(256)S(1)} fusion(bf16[256,4096]{1,0:T(8,128)(2,1)} %param.19), kind=kLoop, calls=%fused_computation | loop fusion | flops 3145472 | bytes 2098176 | tf_op jit(solution)/shard_map/reduce_sum | solution.py:468
  2.9 0.0 copy-done.7
  3.0 0.1 fusion.61
  3.0 0.1 pad_maximum_fusion.3
  3.1 0.0 copy-done.6
  3.1 0.1 fusion.60
  3.2 0.1 pad_maximum_fusion.4
  3.3 0.1 mul.164
  3.4 0.1 mul.159
  3.4 0.1 mul.151
  3.5 0.1 mul.140
  3.6 0.1 broadcast_multiply_fusion.1
  3.7 0.1 copy.35
  3.8 0.1 eq.99
  4.0 0.3 fusion.17
  4.3 0.1 convert_element_type.73
  4.4 0.1 copy.36
  4.5 0.2 fusion.39
  4.8 0.8 copy.37.share_ref
  5.6 0.2 fusion.32
  5.8 0.0 copy-done.2
  5.8 1.3 fusion.14
  7.1 0.2 copy.30
  7.3 0.1 tile.34
  7.4 0.2 copy.34
  7.6 0.1 tile.31
  7.7 0.2 copy.32
  7.9 0.0 copy-start.3
  7.9 1.4 fusion.16
  9.3 0.0 copy-done.3
  9.3 0.8 pad_maximum_fusion.kv_ref
  10.1 1.1 fusion.pick_ref
  11.2 0.1 tile.28
  11.3 0.1 tile.25
  11.4 1.2 fusion.6
  12.7 0.0 copy-start.8
  12.7 0.8 fusion.12
  13.5 0.0 dynamic-slice-start
  13.6 0.1 fusion.34
  13.8 1.3 copy.31
  15.1 2.9 %convolution_convert_fusion = bf16[768,1024]{1,0:T(8,128)(2,1)} fusion(bf16[256,768]{1,0:T(8,128)(2,1)S(1)} %fusion.32, f32[1024]{0:T(1024)S(1)} %dynamic-slice-done, f32[256]{0:T(256)S(1)} %add_rsqrt_fusion, bf16[256,4096]{1,0:T(8,128)(2,1)} %param.19, s32[]{:T(128)} %select_n.106), kind=kOutput, calls=%fused_computation.1 | convolution fusion | flops 404488192 | bytes 2496000 | tf_op jit(solution)/shard_map/dot_general | solution.py:472
  18.0 156.7 %shard_map.140 = (bf16[512,1024]{1,0:T(8,128)(2,1)}, bf16[256,1024]{1,0:T(8,128)(2,1)}) custom-call(bf16[4,1024,128]{2,1,0:T(8,128)(2,1)} %bitcast.68, bf16[2,512,256]{2,1,0:T(8,128)(2,1)} %pad_maximum_fusion.kv_ref, bf16[8,96,1024]{2,1,0:T(8,128)(2,1)} %bitcast.67, bf16[2,256,768]{2,1,0:T(8,128)(2,1)} %fusion.pick_ref, f32[2,256,1]{2,1,0:T(8,128)} %copy.37.share_ref, ...), custom_call_target="tpu_custom_call" | custom-call | tf_op jit(solution)/shard_map/pallas_call | solution.py:494
  174.7 2.3 %copy.48 = bf16[512,1024]{1,0:T(8,128)(2,1)} copy(bf16[512,1024]{1,0:T(8,128)(2,1)} %get-tuple-element.22) | data formatting | bytes 2097152
  177.0 0.0 copy-done.1
  177.0 0.8 copy.49
  (33 shorter events, 0.2 us)
Async XLA Ops:
  0.6 2.3 %copy-start.5 = (f32[256,2]{0,1:T(2,128)S(1)}, f32[256,2]{0,1:T(2,128)}, u32[]{:S(2)}) copy-start(f32[256,2]{0,1:T(2,128)} %param.22) | copy-start | bytes 6148
  0.6 3.1 %copy-start.4 = (s32[256,2]{0,1:T(2,128)S(1)}, s32[256,2]{0,1:T(2,128)}, u32[]{:S(2)}) copy-start(s32[256,2]{0,1:T(2,128)} %param.21) | copy-start | bytes 6148
  0.7 2.5 %copy-start.6 = (f32[64]{0:T(128)S(1)}, f32[64]{0:T(128)}, u32[]{:S(2)}) copy-start(f32[64]{0:T(128)} %param.17) | copy-start | bytes 772
  0.7 2.3 %copy-start.7 = (f32[64]{0:T(128)S(1)}, f32[64]{0:T(128)}, u32[]{:S(2)}) copy-start(f32[64]{0:T(128)} %param.16) | copy-start | bytes 772
  0.7 5.1 %copy-start.2 = (bf16[512,256]{1,0:T(8,128)(2,1)S(1)}, bf16[512,256]{1,0:T(8,128)(2,1)}, u32[]{:S(2)}) copy-start(bf16[512,256]{1,0:T(8,128)(2,1)} %param.14) | copy-start | bytes 786436
  0.7 6.4 %copy-start = (bf16[512,512]{1,0:T(8,128)(2,1)S(1)}, bf16[512,512]{1,0:T(8,128)(2,1)}, u32[]{:S(2)}) copy-start(bf16[512,512]{1,0:T(8,128)(2,1)} %param.13) | copy-start | bytes 1572868
  7.9 1.4 copy-start.3
  12.7 0.9 copy-start.8
  13.5 1.6 dynamic-slice-start
  174.7 2.3 %copy-start.1 = (bf16[256,1024]{1,0:T(8,128)(2,1)S(1)}, bf16[256,1024]{1,0:T(8,128)(2,1)}, u32[]{:S(2)}) copy-start(bf16[256,1024]{1,0:T(8,128)(2,1)} %get-tuple-element.23) | copy-start | bytes 1572868
where the time goes:
time: 178 us
  Pallas kernels  157 us (88%)
  matrix products  7.79 us (4%)
  local copies, waits for them, and re-layouts  7.35 us (4%)
  other arithmetic  4.95 us (3%)
    pallas_call x1, Pallas kernels, on_device(): pl.pallas_call(functools.partial(kernel, (n, T, head_width, hp)), out_sha...  157 us
    unnamed x28, local copies, waits for them, and re-layouts  3.57 us

commit v1 on v0

v1 whole, which is shorter than its diff:
```python
import functools
import math

import jax
import jax.numpy as jnp
from jax import lax
from jax.experimental import pallas as pl
from jax.experimental.pallas import tpu as pltpu
from jax.sharding import PartitionSpec as P

GRID_W = 64
CORES = 2
ONES = 16

epsilon = 1e-06
base_theta = 10000.0


def rope_tables(first_row, grid_rows, head_width, width):
    quarter = head_width // 4
    lane = jnp.arange(width, dtype=jnp.int32)
    inverse = base_theta ** (-(lane % quarter).astype(jnp.float32) / quarter)
    line = jnp.arange(grid_rows + GRID_W, dtype=jnp.int32)
    place = jnp.where(line < grid_rows, first_row + line, line - grid_rows)
    angles = place.astype(jnp.float32)[:, None] * inverse[None, :]
    first = (lane % head_width) < head_width // 2
    sine = jnp.sin(angles)
    return jnp.cos(angles), jnp.where(first[None, :], -sine, sine)


def norm_rotate(columns, gain, gain_swapped, cosine, sine, head_width):
    width = columns.shape[1]
    a = lax.broadcasted_iota(jnp.int32, (width, width), 0)
    b = lax.broadcasted_iota(jnp.int32, (width, width), 1)
    half = head_width // 2
    same_head = jnp.where(a // head_width == b // head_width, 1.0, 0.0)
    partner = jnp.where(b % head_width < half, b + half, b - half)
    swap = jnp.where(a == partner, 1.0, 0.0).astype(jnp.bfloat16)
    values = columns.astype(jnp.float32)
    mean = (
        jnp.dot(
            values * values,
            same_head,
            precision=lax.Precision.HIGHEST,
            preferred_element_type=jnp.float32,
        )
        / head_width
    )
    scale = lax.rsqrt(mean + epsilon)
    swapped = jnp.dot(columns, swap, preferred_element_type=jnp.float32)
    return (
        values * scale * gain * cosine + swapped * scale * gain_swapped * sine
    ).astype(jnp.bfloat16)


def kernel(
    dims,
    x_hbm,
    q_hbm,
    k_hbm,
    v_hbm,
    gate_hbm,
    up_hbm,
    down_hbm,
    mixer_hbm,
    cos_table,
    sin_table,
    q_gain_ref,
    k_gain_ref,
    moe_gain_ref,
    rows_ref,
    weight_ref,
    attn_ref,
    moe_ref,
    x_in,
    q_in,
    k_in,
    v_in,
    normed,
    disp,
    near,
    pick,
    share_ref,
    cos_ref,
    sin_ref,
    q_all,
    k_all,
    v_all,
    incoming,
    hid,
    eo,
    ret,
    att_all,
    mix_acc,
    gate_w,
    up_w,
    down_w,
    mixer_w,
    m_ref,
    acc_ref,
    w_sem,
    d_send,
    d_recv,
    near_sem,
    kv_up,
    kv_down,
    kv_recv,
    f_send,
    f_recv,
    g_send,
    g_recv,
    h_send,
    h_recv,
    r_send,
    r_recv,
    a_send,
    a_recv,
):
    n, T, head_width = dims
    nz = n // CORES
    e = lax.axis_index("ep")
    t = lax.axis_index("tp")
    z = e // CORES
    c = e % CORES
    sibling = z * CORES + (1 - c)
    kh, group_rows, pw = q_all.shape
    rows = q_in.shape[0]
    group = group_rows // rows
    gw = group * head_width
    kw = k_in.shape[1]
    token_count, model_width = x_in.shape
    top = rows_ref.shape[0]
    capp = disp.shape[1]
    feat = disp.shape[2]
    ffl = gate_w.shape[1]
    cols = down_w.shape[1]
    bf = jnp.bfloat16
    f32 = jnp.float32

    loads = [
        pltpu.make_async_copy(src, dst, w_sem.at[i])
        for i, (src, dst) in enumerate(
            [
                (x_hbm, x_in),
                (k_hbm, k_in),
                (v_hbm, v_in),
                (q_hbm, q_in),
                (gate_hbm, gate_w),
                (up_hbm, up_w),
                (down_hbm, down_w),
                (mixer_hbm, mixer_w),
            ]
        )
    ]
    for load in loads:
        load.start()

    barrier = pltpu.get_barrier_semaphore()

    def greet(j, carry):
        pl.semaphore_signal(
            barrier, inc=1, device_id={"ep": (e + j) % n}, device_id_type=pl.DeviceIdType.MESH
        )
        return carry

    lax.fori_loop(1, n, greet, 0)
    for p in range(1, T):
        pl.semaphore_signal(
            barrier, inc=1, device_id={"tp": (t + p) % T}, device_id_type=pl.DeviceIdType.MESH
        )

    low = jnp.minimum(z, nz - 1 - z)
    left = z * 2 < nz

    inner = low > 0

    def line(k):
        outward = ((k + 1) // 2) * (2 * (k % 2) - 1)
        around = jnp.where(left, z - outward, z + outward)
        return jnp.where(k <= 2 * low, around, jnp.where(left, k, nz - 1 - k))

    def chip(k):
        if nz != 4:
            return line(k)
        near = jnp.where(k == 2, 3, jnp.where(k == 3, 2, k))
        return line(jnp.where(inner, near, jnp.where(k == 0, 0, k % 3 + 1)))

    def rdma(src, dst, ss, rs, axis, index):
        return pltpu.make_async_remote_copy(
            src_ref=src,
            dst_ref=dst,
            send_sem=ss,
            recv_sem=rs,
            device_id={axis: index},
            device_id_type=pl.DeviceIdType.MESH,
        )

    class Swap:
        def __init__(self, view, send, recv, k):
            self.view, self.send, self.recv, self.k = view, send, recv, k

        def copy(self, slot, owner, half, peer):
            block = self.view(owner, half)
            return rdma(
                block, block, self.send.at[slot, self.k], self.recv.at[slot, self.k], "tp", peer
            )

        def plan(self):
            x_next, y_next = t + 1 - 2 * (t % 2), (t + 2) % 4
            return [
                (0, t, None, x_next),
                (1, t, None, y_next),
                (2, x_next, 0, y_next),
                (3, y_next, 1, x_next),
            ]

        def start(self):
            if T == 4:
                for slot, owner, half, peer in self.plan()[:2]:
                    self.copy(slot, owner, half, peer).start()
            else:
                for p in range(1, T):
                    self.copy(p - 1, t, None, (t + p) % T).start()

        def relay(self):
            if T == 4:
                x_next, y_next = t + 1 - 2 * (t % 2), (t + 2) % 4
                for first, owner, plan in (
                    (0, x_next, self.plan()[2]),
                    (1, y_next, self.plan()[3]),
                ):
                    self.copy(first, owner, None, owner).wait_recv()
                    self.copy(*plan).start()

        def finish(self):
            if T == 4:
                for slot in (2, 3):
                    self.copy(slot, 3 - t, slot - 2, 3 - t).wait_recv()
            else:
                for p in range(1, T):
                    owner = (t + T - p) % T
                    self.copy(p - 1, owner, None, owner).wait_recv()

        def drain(self):
            if T == 4:
                for slot, owner, half, peer in self.plan():
                    self.copy(slot, owner, half, peer).wait_send()
            else:
                for p in range(1, T):
                    self.copy(p - 1, t, None, (t + p) % T).wait_send()

    def pair_at(k):
        return pl.ds(chip(k) * CORES, CORES)

    def pair_view(buffer, k):
        def view(owner, half):
            if half is None:
                return buffer.at[owner, pair_at(k)]
            return buffer.at[owner, chip(k) * CORES + half]

        return view

    def g_swap(k):
        return Swap(pair_view(incoming, k), g_send, g_recv, k)

    def h_swap(k):
        return Swap(pair_view(hid, k), h_send, h_recv, k)

    def att_view(owner, half):
        if half is None:
            return att_all.at[owner]
        return att_all.at[owner, pl.ds(half * (rows // 2), rows // 2)]

    a_swap = Swap(att_view, a_send, a_recv, 0)

    def d_copy(dest, origin):
        return rdma(
            disp.at[dest], incoming.at[t, origin], d_send.at[dest], d_recv.at[origin], "ep", dest
        )

    near_copy = rdma(near, incoming.at[:, e], near_sem.at[0], near_sem.at[1], "ep", sibling)
    near_in = rdma(near, incoming.at[:, sibling], near_sem.at[0], near_sem.at[1], "ep", sibling)

    def kv_copies(zk, core, send, recv, dest):
        at = pl.ds(pl.multiple_of(core * rows, rows), rows)
        keys = k_all.at[zk, at]
        values = v_all.at[zk, :, 0:head_width, at]
        return [
            rdma(keys, keys, send.at[0, zk], recv.at[0, zk], "ep", dest),
            rdma(values, values, send.at[1, zk], recv.at[1, zk], "ep", dest),
        ]

    def kv_step(zk, direction):
        send = kv_up if direction > 0 else kv_down
        return kv_copies(zk, c, send, kv_recv, (e + direction * CORES + n) % n)

    def kv_across(zk):
        return kv_copies(zk, c, f_send, f_recv, sibling)

    def kv_pass(zk, act):
        @pl.when((zk <= z) & (z + 1 < nz))
        def _():
            for copy in kv_step(zk, 1):
                act(copy)

        @pl.when((zk >= z) & (z > 0))
        def _():
            for copy in kv_step(zk, -1):
                act(copy)

        for copy in kv_across(zk):
            act(copy)

    def places():
        expert = lax.broadcasted_iota(jnp.int32, (n, token_count), 0)
        named = [expert == rows_ref[k : k + 1, :] for k in range(top)]
        count = sum(jnp.where(x, 1.0, 0.0) for x in named).astype(bf)
        i = lax.broadcasted_iota(jnp.int32, (token_count, token_count), 0)
        j = lax.broadcasted_iota(jnp.int32, (token_count, token_count), 1)
        earlier = jnp.dot(
            count, jnp.where(i < j, 1.0, 0.0).astype(bf), preferred_element_type=f32
        )
        by_row = [
            rows_ref[k : k + 1, :].astype(f32) * capp
            + jnp.sum(jnp.where(named[k], earlier, 0.0), axis=0, keepdims=True)
            for k in range(top)
        ]
        width = 128
        weights = [weight_ref[k : k + 1, :] for k in range(top)]
        total = sum(weights)
        lines = by_row + [x / total for x in weights]
        lines.append(jnp.zeros((width - len(lines), token_count), f32))
        by_col = jnp.concatenate(lines, axis=0).T
        return by_row, by_col

    table_width = cos_table.shape[1]
    grid_rows = rows // GRID_W
    lane = lax.broadcasted_iota(jnp.int32, (GRID_W, table_width), 1)
    by_grid_row = (lane // (head_width // 4)) % 2 == 0
    for table, out in ((cos_table, cos_ref), (sin_table, sin_ref)):
        for r in range(grid_rows):
            out[r * GRID_W : (r + 1) * GRID_W] = jnp.where(
                by_grid_row, table[r : r + 1], table[grid_rows:]
            )

    def gain_rows(ref, width):
        gain = ref[...]
        flipped = [gain[:, head_width // 2 :], gain[:, : head_width // 2]]
        times = width // head_width
        return (
            jnp.concatenate([gain] * times, axis=1) if times > 1 else gain,
            jnp.concatenate(flipped * times, axis=1),
        )

    q_gain, q_gain_swapped = gain_rows(q_gain_ref, gw)
    k_gain, k_gain_swapped = gain_rows(k_gain_ref, pw)

    by_row, by_col = places()

    loads[0].wait()
    strip = math.gcd(token_count, 64)

    def normalise(i, carry):
        at = pl.ds(pl.multiple_of(i * strip, strip), strip)
        values = x_in[at].astype(f32)
        inv = lax.rsqrt(jnp.mean(values * values, axis=1, keepdims=True) + epsilon)
        normed[at] = (values * inv * moe_gain_ref[...]).astype(bf)
        return carry

    lax.fori_loop(0, token_count // strip, normalise, 0)

    def chosen(first, count):
        slot = lax.broadcasted_iota(jnp.int32, (count, token_count), 0).astype(f32)
        slot = slot + (first * capp).astype(f32)
        return sum(jnp.where(slot == place, 1.0, 0.0) for place in by_row).astype(bf)

    pl.semaphore_wait(barrier, n - 1 + T - 1)
    own_features = pl.ds(pl.multiple_of(t * feat, feat), feat)

    def make_disp(k, carry):
        part = jnp.dot(
            chosen(chip(k) * CORES, CORES * capp),
            normed[:, own_features],
            preferred_element_type=f32,
        ).astype(bf)
        disp[pair_at(k)] = part.reshape(CORES, capp, feat)
        return carry

    def send_disp(i, carry):
        k = jnp.where(i == 1, 1, nz + 1 - i)
        for cc in range(CORES):
            d_copy(line(k) * CORES + cc, e).start()
        return carry

    lax.fori_loop(1, nz, make_disp, 0)
    lax.fori_loop(1, nz, send_disp, 0)
    loads[1].wait()
    loads[2].wait()
    own_keys = pl.ds(pl.multiple_of(c * rows, rows), rows)
    for p in range(kw // pw):
        lanes = slice(p * pw, (p + 1) * pw)
        k_all[z, own_keys, lanes] = norm_rotate(
            k_in[:, lanes],
            k_gain,
            k_gain_swapped,
            cos_ref[:, :pw],
            sin_ref[:, :pw],
            head_width,
        )
        turned = v_in[:, lanes].astype(f32).T.astype(bf)
        for i in range(pw // head_width):
            v_all[z, p * (pw // head_width) + i, 0:head_width, own_keys] = turned[
                i * head_width : (i + 1) * head_width
            ]

    kv_pass(z, lambda copy: copy.start())

    own_pick = chosen(e, capp)
    sibling_pick = chosen(sibling, capp)
    for s in range(T):
        at = slice(s * feat, (s + 1) * feat)
        near[s] = jnp.dot(sibling_pick, normed[:, at], preferred_element_type=f32).astype(bf)
    near_copy.start()
    for s in range(T):
        at = slice(s * feat, (s + 1) * feat)
        incoming[s, e] = jnp.dot(own_pick, normed[:, at], preferred_element_type=f32).astype(bf)

    def spread(k):
        for cc in range(CORES):
            d_copy(chip(k) * CORES + cc, chip(k) * CORES + cc).wait_recv()
        g_swap(k).start()

    v_all[:, :, head_width:, :] = jnp.ones(
        (nz, kh, v_all.shape[2] - head_width, CORES * rows), bf
    )
    m_ref[...] = jnp.full(m_ref.shape, -jnp.inf, f32)
    acc_ref[...] = jnp.zeros(acc_ref.shape, f32)
    slots = lax.broadcasted_iota(jnp.int32, (token_count, n * capp), 1).astype(f32)
    for k in range(top):
        pick[k] = jnp.where(slots == by_col[:, k : k + 1], 1.0, 0.0).astype(bf)
        share_ref[k] = by_col[:, top + k : top + k + 1]

    loads[3].wait()
    for h in range(kh):
        turned = norm_rotate(
            q_in[:, h * gw : (h + 1) * gw],
            q_gain,
            q_gain_swapped,
            cos_ref[:, :gw],
            sin_ref[:, :gw],
            head_width,
        )
        place = (h * head_width) % pw
        for g in range(group):
            parts = [turned[:, g * head_width : (g + 1) * head_width]]
            if place:
                parts.insert(0, jnp.zeros((rows, place), bf))
            if pw - place - head_width:
                parts.append(jnp.zeros((rows, pw - place - head_width), bf))
            q_all[h, g * rows : (g + 1) * rows] = (
                jnp.concatenate(parts, axis=1) if len(parts) > 1 else parts[0]
            )

    factor = math.log2(math.e) * head_width ** (-0.5)
    step_rows = math.gcd(group_rows, 512)

    def attend(zk):
        def one_head(h, carry):
            lanes = pl.ds(pl.multiple_of((h * head_width) // pw * pw, pw), pw)
            keys = k_all[zk, :, lanes] if kh > 1 else k_all[zk]
            values = v_all[zk, h]

            def scores_at(r):
                return lax.dot_general(
                    keys,
                    q_all[h, r : r + step_rows],
                    (((1,), (1,)), ((), ())),
                    preferred_element_type=f32,
                )

            later = scores_at(0)
            for r in range(0, group_rows, step_rows):
                scores = later
                if r + step_rows < group_rows:
                    later = scores_at(r + step_rows)
                at = slice(r, r + step_rows)
                old = m_ref[h, :, at]
                new = jnp.maximum(old, jnp.max(scores, axis=0, keepdims=True))
                weights = jnp.exp2(scores * factor - new * factor).astype(bf)
                m_ref[h, :, at] = new
                acc_ref[h, :, at] = acc_ref[h, :, at] * jnp.exp2((old - new) * factor) + jnp.dot(
                    values, weights, preferred_element_type=f32
                )
            return carry

        lax.fori_loop(0, kh, one_head, 0)

    def kv_arrive(k):
        zk = line(k)

        @pl.when(zk != z)
        def _():
            for copy in kv_step(zk, 1):
                copy.wait_recv()
            kv_pass(zk, lambda copy: copy.start())

    def kv_join(k):
        for copy in kv_copies(line(k), 1 - c, f_send, f_recv, sibling):
            copy.wait_recv()

    def first_half(k):
        @pl.when(k == 0)
        def _():
            near_in.wait_recv()

        @pl.when(k > 0)
        def _():
            g_swap(k).finish()

        gate = jnp.zeros((CORES * capp, ffl), f32)
        up = jnp.zeros((CORES * capp, ffl), f32)
        for s in range(T):
            piece = incoming[s, pair_at(k)].reshape(CORES * capp, feat)
            at = slice(s * feat, (s + 1) * feat)
            gate = gate + jnp.dot(piece, gate_w[at], preferred_element_type=f32)
            up = up + jnp.dot(piece, up_w[at], preferred_element_type=f32)
        hidden = (gate / (1.0 + jnp.exp(-gate)) * up).astype(bf)
        hid[t, pair_at(k)] = hidden.reshape(CORES, capp, ffl)
        h_swap(k).start()

    def r_copy(dest, origin):
        return rdma(eo.at[dest], ret.at[origin], r_send.at[dest], r_recv.at[origin], "ep", dest)

    def second_half(k):
        h_swap(k).finish()
        total = jnp.zeros((CORES * capp, cols), f32)
        for s in range(T):
            piece = hid[s, pair_at(k)].reshape(CORES * capp, ffl)
            total = total + jnp.dot(
                piece, down_w[s * ffl : (s + 1) * ffl], preferred_element_type=f32
            )
        eo[pair_at(k)] = total.astype(bf).reshape(CORES, capp, cols)

    def send_back(k):
        for cc in range(CORES):
            origin = chip(k) * CORES + cc

            @pl.when(origin != e)
            def _():
                r_copy(origin, e).start()

            @pl.when(origin == e)
            def _():
                ret[origin] = eo[origin]

    def tuned():
        outer = jnp.logical_not(inner)
        spread(1)
        kv_join(0)
        attend(z)
        for load in loads[4:7]:
            load.wait()
        first_half(0)
        g_swap(1).relay()
        spread(2)
        h_swap(0).relay()
        first_half(1)
        spread(3)
        g_swap(2).relay()
        second_half(0)
        send_back(0)
        h_swap(1).relay()
        kv_arrive(1)
        g_swap(3).relay()

        @pl.when(inner)
        def _():
            kv_arrive(2)

        first_half(2)
        second_half(1)
        kv_join(1)
        attend(line(1))

        @pl.when(inner)
        def _():
            kv_arrive(3)

        h_swap(2).relay()
        first_half(3)
        second_half(2)

        @pl.when(inner)
        def _():
            send_back(1)

        @pl.when(outer)
        def _():
            kv_arrive(2)

        h_swap(3).relay()
        second_half(3)
        send_back(3)
        kv_join(2)
        attend(line(2))
        send_back(2)

        @pl.when(outer)
        def _():
            send_back(1)
            kv_arrive(3)

        kv_join(3)
        attend(line(3))

    def general():
        kv_join(0)
        attend(z)
        for load in loads[4:7]:
            load.wait()
        if nz > 1:
            spread(1)

        def step(j, carry):
            @pl.when(j < nz)
            def _():
                first_half(j)

            @pl.when(j + 1 < nz)
            def _():
                g_swap(j + 1).relay()

            @pl.when(j + 2 < nz)
            def _():
                spread(j + 2)

            @pl.when((j >= 1) & (j < nz))
            def _():
                kv_arrive(j)

            @pl.when(j >= 1)
            def _():
                h_swap(j - 1).relay()

            @pl.when(j >= 2)
            def _():
                kv_join(j - 1)
                attend(line(j - 1))

            @pl.when(j >= 1)
            def _():
                second_half(j - 1)
                send_back(j - 1)

            return carry

        lax.fori_loop(0, nz + 1, step, 0)

    if nz == 4:
        tuned()
    else:
        general()

    for h in range(kh):
        done = acc_ref[h, 0:head_width] / acc_ref[h, head_width : head_width + 1]
        done = jnp.concatenate([done[:, g * rows : (g + 1) * rows] for g in range(group)], axis=0)
        att_all[t, :, h * gw : (h + 1) * gw] = done.T.astype(bf)
    a_swap.start()

    loads[7].wait()
    aw = att_all.shape[2]
    out_cols = attn_ref.shape[1]
    half = math.gcd(out_cols, 256)

    def mix(owners, opening, closing):
        def strip_of(i, carry):
            at = pl.ds(pl.multiple_of(i * half, half), half)
            total = jnp.zeros((rows, half), f32) if opening else mix_acc[:, at]
            for s in owners:
                total = total + jnp.dot(
                    att_all[s],
                    mixer_w[pl.ds(pl.multiple_of(s * aw, aw), aw), at],
                    preferred_element_type=f32,
                )
            if closing:
                attn_ref[:, at] = total.astype(bf)
            else:
                mix_acc[:, at] = total
            return carry

        lax.fori_loop(0, out_cols // half, strip_of, 0)

    def gather_experts():
        def wait_ret(j, carry):
            origin = (e + j) % n
            r_copy(origin, origin).wait_recv()
            return carry

        lax.fori_loop(1, n, wait_ret, 0)
        returned = ret[...].reshape(n * capp, cols)
        combined = jnp.zeros(moe_ref.shape, f32)
        for k in range(top):
            combined = combined + share_ref[k] * jnp.dot(
                pick[k], returned, preferred_element_type=f32
            )
        moe_ref[...] = combined.astype(bf)

    mix([t], True, False)
    a_swap.relay()
    if T == 4:
        mix([t + 1 - 2 * (t % 2), (t + 2) % 4], False, False)
    gather_experts()
    a_swap.finish()
    if T == 4:
        mix([3 - t], False, True)
    else:
        mix([(t + p) % T for p in range(1, T)], False, True)

    near_copy.wait_send()

    def drain_ep(j, carry):
        r_copy((e + j) % n, e).wait_send()
        return carry

    lax.fori_loop(1, n, drain_ep, 0)

    def drain(k, carry):
        kv_pass(k, lambda copy: copy.wait_send())
        h_swap(k).drain()

        @pl.when(k > 0)
        def _():
            g_swap(k).drain()
            for cc in range(CORES):
                d_copy(chip(k) * CORES + cc, e).wait_send()

        return carry

    lax.fori_loop(0, nz, drain, 0)
    a_swap.drain()


def on_device(
    n,
    T,
    query_input,
    key_input,
    value_input,
    query_gain,
    key_gain,
    mixer_out,
    moe_input,
    moe_gain,
    routes,
    route_weight,
    expert_gate,
    expert_up,
    expert_down,
):
    rows = query_input.shape[0]
    head_width = query_gain.shape[0]
    heads_here = query_input.shape[1] // head_width
    kw = key_input.shape[1]
    kh = kw // head_width
    group = heads_here // kh
    pw = min(128, kw)
    gw = group * head_width
    width = max(gw, pw)
    assert rows % GRID_W == 0
    grid_rows = rows // GRID_W
    cosine, sine = rope_tables(lax.axis_index("ep") * grid_rows, grid_rows, head_width, width)

    token_count, model_width = moe_input.shape
    top = routes.shape[1]
    local_experts = expert_gate.shape[0]
    assert local_experts == 1
    expert_count = local_experts * n
    capacity = 3 * token_count * top // (2 * expert_count)
    capp = -(-capacity // 16) * 16
    feat = model_width // T
    gate = expert_gate[0]
    up = expert_up[0]
    down = expert_down[0]
    ffl = gate.shape[1]
    cols = down.shape[1]
    nz = n // CORES
    aw = heads_here * head_width
    out_cols = mixer_out.shape[1]
    slots = 4 if T == 4 else T - 1
    bf = jnp.bfloat16
    dma = pltpu.SemaphoreType.DMA
    vmem = pl.BlockSpec(memory_space=pltpu.VMEM)
    hbm = pl.BlockSpec(memory_space=pl.ANY)
    return pl.pallas_call(
        functools.partial(kernel, (n, T, head_width)),
        out_shape=(
            jax.ShapeDtypeStruct((rows, out_cols), bf),
            jax.ShapeDtypeStruct((token_count, cols), bf),
        ),
        in_specs=[hbm] * 8 + [vmem] * 7,
        out_specs=(vmem, vmem),
        scratch_shapes=[
            pltpu.VMEM(moe_input.shape, bf),
            pltpu.VMEM(query_input.shape, bf),
            pltpu.VMEM(key_input.shape, bf),
            pltpu.VMEM(value_input.shape, bf),
            pltpu.VMEM(moe_input.shape, bf),
            pltpu.VMEM((n, capp, feat), bf),
            pltpu.VMEM((T, capp, feat), bf),
            pltpu.VMEM((top, token_count, n * capp), bf),
            pltpu.VMEM((top, token_count, 1), jnp.float32),
            pltpu.VMEM((rows, width), jnp.float32),
            pltpu.VMEM((rows, width), jnp.float32),
            pltpu.VMEM((kh, group * rows, pw), bf),
            pltpu.VMEM((nz, CORES * rows, kw), bf),
            pltpu.VMEM((nz, kh, head_width + ONES, CORES * rows), bf),
            pltpu.VMEM((T, n, capp, feat), bf),
            pltpu.VMEM((T, n, capp, ffl), bf),
            pltpu.VMEM((n, capp, cols), bf),
            pltpu.VMEM((n, capp, cols), bf),
            pltpu.VMEM((T, rows, aw), bf),
            pltpu.VMEM((rows, out_cols), jnp.float32),
            pltpu.VMEM(gate.shape, bf),
            pltpu.VMEM(up.shape, bf),
            pltpu.VMEM(down.shape, bf),
            pltpu.VMEM(mixer_out.shape, bf),
            pltpu.VMEM((kh, 1, group * rows), jnp.float32),
            pltpu.VMEM((kh, head_width + ONES, group * rows), jnp.float32),
            dma((8,)),
            dma((n,)),
            dma((n,)),
            dma((2,)),
            dma((2, nz)),
            dma((2, nz)),
            dma((2, nz)),
            dma((2, nz)),
            dma((2, nz)),
            dma((slots, nz)),
            dma((slots, nz)),
            dma((slots, nz)),
            dma((slots, nz)),
            dma((n,)),
            dma((n,)),
            dma((slots, 1)),
            dma((slots, 1)),
        ],
        compiler_params=pltpu.CompilerParams(
            collective_id=0, has_side_effects=True, vmem_limit_bytes=63 * 1024 * 1024
        ),
    )(
        moe_input,
        query_input,
        key_input,
        value_input,
        gate,
        up,
        down,
        mixer_out,
        cosine,
        sine,
        query_gain[None, :],
        key_gain[None, :],
        moe_gain[None, :],
        routes.T,
        route_weight.T,
    )


def solution(mesh):
    placed = (
        P("ep", "tp"),
        P("ep", "tp"),
        P("ep", "tp"),
        P(),
        P(),
        P(None, "tp"),
        P("ep", None),
        P(),
        P("ep", None),
        P("ep", None),
        P("ep", None, "tp"),
        P("ep", None, "tp"),
        P("ep", None, "tp"),
    )
    return jax.shard_map(
        functools.partial(on_device, mesh.shape["ep"], mesh.shape["tp"]),
        mesh=mesh,
        in_specs=placed,
        out_specs=(P("ep", "tp"), P("ep", "tp")),
        check_vma=False,
    )
```

time: 178 us -> 126 us (0.71)
  the two profiles are of different devices: /device:TPU:12 before, /device:TPU:0 now
where the time goes in v1:
time: 126 us
  Pallas kernels  121 us (96%)
  local copies, waits for them, and re-layouts  3.12 us (2%)
    pallas_call x1, Pallas kernels, on_device(): pl.pallas_call(functools.partial(kernel, (n, T, head_width)), out_shape=(...  121 us
    unnamed x4, local copies, waits for them, and re-layouts  3.12 us

profile of v1, /device:TPU:0, one launch (start us, length us, event | category | flops | bytes accessed | tf_op | source)
XLA Modules:
  0.0 126.0 jit_solution(2339062695154658002)
XLA Ops:
  0.7 0.8 negate_select_fusion
  1.5 121.4 %shard_map.140 = (bf16[512,1024]{1,0:T(8,128)(2,1)}, bf16[256,1024]{1,0:T(8,128)(2,1)}) custom-call(bf16[256,4096]{1,0:T(8,128)(2,1)} %x_hbm.1, bf16[512,512]{1,0:T(8,128)(2,1)} %q_hbm.1, bf16[512,256]{1,0:T(8,128)(2,1)} %k_hbm.1, bf16[512,256]{1,0:T(8,128)(2,1)} %v_hbm.1, bf16[4096,256]{1,0:T(8,128)(2,1)} %bitcast.8, bf16[4096,256]{1,0:T(8,128)(2,1)} %bitcast.9, ...), custom_call_target="tpu_custom_call" | custom-call | tf_op jit(solution)/shard_map/pallas_call | solution.py:794
  122.9 0.0 copy-start
  122.9 2.3 %copy.17 = bf16[512,1024]{1,0:T(8,128)(2,1)} copy(bf16[512,1024]{1,0:T(8,128)(2,1)} %get-tuple-element.6) | data formatting | bytes 2097152
  125.2 0.0 copy-done
  125.2 0.8 copy.18
  (3 shorter events, 0.0 us)
Async XLA Ops:
  122.9 2.3 %copy-start = (bf16[256,1024]{1,0:T(8,128)(2,1)S(1)}, bf16[256,1024]{1,0:T(8,128)(2,1)}, u32[]{:S(2)}) copy-start(bf16[256,1024]{1,0:T(8,128)(2,1)} %get-tuple-element.7) | copy-start | bytes 1572868

commit v2 on v1

--- a/solution.py
+++ b/solution.py
@@ -70,8 +70,11 @@
     moe_gain_ref,
     rows_ref,
     weight_ref,
+    attn_hbm,
+    moe_hbm,
     attn_ref,
     moe_ref,
+    o_sem,
     x_in,
     q_in,
     k_in,
@@ -266,12 +269,13 @@
     def h_swap(k):
         return Swap(pair_view(hid, k), h_send, h_recv, k)
 
-    def att_view(owner, half):
-        if half is None:
-            return att_all.at[owner]
-        return att_all.at[owner, pl.ds(half * (rows // 2), rows // 2)]
-
-    a_swap = Swap(att_view, a_send, a_recv, 0)
+    def a_swap(part):
+        def view(owner, half):
+            if half is None:
+                return att_all.at[owner, part]
+            return att_all.at[owner, part, pl.ds(half * (rows // 2), rows // 2)]
+
+        return Swap(view, a_send, a_recv, part)
 
     def d_copy(dest, origin):
         return rdma(
@@ -464,7 +468,10 @@
     factor = math.log2(math.e) * head_width ** (-0.5)
     step_rows = math.gcd(group_rows, 512)
 
-    def attend(zk):
+    parts = att_all.shape[1]
+    heads_part = kh // parts
+
+    def attend(zk, first=0, last=kh):
         def one_head(h, carry):
             lanes = pl.ds(pl.multiple_of((h * head_width) // pw * pw, pw), pw)
             keys = k_all[zk, :, lanes] if kh > 1 else k_all[zk]
@@ -493,7 +500,7 @@
                 )
             return carry
 
-        lax.fori_loop(0, kh, one_head, 0)
+        lax.fori_loop(first, last, one_head, 0)
 
     def kv_arrive(k):
         zk = line(k)
@@ -552,6 +559,16 @@
             @pl.when(origin == e)
             def _():
                 ret[origin] = eo[origin]
+
+    def finish_heads(part):
+        for i in range(heads_part):
+            h = part * heads_part + i
+            done = acc_ref[h, 0:head_width] / acc_ref[h, head_width : head_width + 1]
+            done = jnp.concatenate(
+                [done[:, g * rows : (g + 1) * rows] for g in range(group)], axis=0
+            )
+            att_all[t, part, :, i * gw : (i + 1) * gw] = done.T.astype(bf)
+        a_swap(part).start()
 
     def tuned():
         outer = jnp.logical_not(inner)
@@ -571,47 +588,60 @@
         send_back(0)
         h_swap(1).relay()
         kv_arrive(1)
+        kv_join(1)
+        attend(line(1), 0, kh // 2)
+
+        @pl.when(inner)
+        def _():
+            kv_arrive(2)
+
+        @pl.when(outer)
+        def _():
+            attend(line(1), kh // 2, kh)
+
         g_swap(3).relay()
 
         @pl.when(inner)
         def _():
-            kv_arrive(2)
+            attend(line(1), kh // 2, kh)
 
         first_half(2)
         second_half(1)
-        kv_join(1)
-        attend(line(1))
 
         @pl.when(inner)
         def _():
             kv_arrive(3)
+            send_back(1)
 
         h_swap(2).relay()
         first_half(3)
+
+        @pl.when(outer)
+        def _():
+            send_back(1)
+
         second_half(2)
 
-        @pl.when(inner)
-        def _():
-            send_back(1)
-
         @pl.when(outer)
         def _():
             kv_arrive(2)
 
         h_swap(3).relay()
+        kv_join(2)
+        attend(line(2), 0, kh // 2)
         second_half(3)
         send_back(3)
-        kv_join(2)
-        attend(line(2))
+        attend(line(2), kh // 2, kh)
         send_back(2)
 
         @pl.when(outer)
         def _():
-            send_back(1)
             kv_arrive(3)
 
         kv_join(3)
-        attend(line(3))
+        for part in range(parts):
+            attend(line(3), part * heads_part, (part + 1) * heads_part)
+            finish_heads(part)
 
     def general():
         kv_join(0)
@@ -655,35 +685,39 @@
             return carry
 
         lax.fori_loop(0, nz + 1, step, 0)
+        for part in range(parts):
+            finish_heads(part)
 
     if nz == 4:
         tuned()
     else:
         general()
 
-    for h in range(kh):
-        done = acc_ref[h, 0:head_width] / acc_ref[h, head_width : head_width + 1]
-        done = jnp.concatenate([done[:, g * rows : (g + 1) * rows] for g in range(group)], axis=0)
-        att_all[t, :, h * gw : (h + 1) * gw] = done.T.astype(bf)
-    a_swap.start()
-
     loads[7].wait()
-    aw = att_all.shape[2]
+    aw = parts * att_all.shape[3]
     out_cols = attn_ref.shape[1]
     half = math.gcd(out_cols, 256)
+
+    def strip_out(i):
+        at = pl.ds(pl.multiple_of(i * half, half), half)
+        return pltpu.make_async_copy(attn_ref.at[:, at], attn_hbm.at[:, at], o_sem.at[i + 1])
+
+    moe_out = pltpu.make_async_copy(moe_ref, moe_hbm, o_sem.at[0])
 
     def mix(owners, opening, closing):
         def strip_of(i, carry):
             at = pl.ds(pl.multiple_of(i * half, half), half)
             total = jnp.zeros((rows, half), f32) if opening else mix_acc[:, at]
             for s in owners:
-                total = total + jnp.dot(
-                    att_all[s],
-                    mixer_w[pl.ds(pl.multiple_of(s * aw, aw), aw), at],
-                    preferred_element_type=f32,
-                )
+                for part in range(parts):
+                    width = aw // parts
+                    lines = pl.ds(pl.multiple_of(s * aw + part * width, width), width)
+                    total = total + jnp.dot(
+                        att_all[s, part], mixer_w[lines, at], preferred_element_type=f32
+                    )
             if closing:
                 attn_ref[:, at] = total.astype(bf)
+                strip_out(i).start()
             else:
                 mix_acc[:, at] = total
             return carry
@@ -704,13 +738,16 @@
                 pick[k], returned, preferred_element_type=f32
             )
         moe_ref[...] = combined.astype(bf)
+        moe_out.start()
 
     mix([t], True, False)
-    a_swap.relay()
+    for part in range(parts):
+        a_swap(part).relay()
     if T == 4:
         mix([t + 1 - 2 * (t % 2), (t + 2) % 4], False, False)
     gather_experts()
-    a_swap.finish()
+    for part in range(parts):
+        a_swap(part).finish()
     if T == 4:
         mix([3 - t], False, True)
     else:
@@ -737,7 +774,15 @@
         return carry
 
     lax.fori_loop(0, nz, drain, 0)
-    a_swap.drain()
+    for part in range(parts):
+        a_swap(part).drain()
+    moe_out.wait()
+
+    def drain_out(i, carry):
+        strip_out(i).wait()
+        return carry
+
+    lax.fori_loop(0, out_cols // half, drain_out, 0)
 
 
 def on_device(
@@ -787,6 +832,7 @@
     aw = heads_here * head_width
     out_cols = mixer_out.shape[1]
     slots = 4 if T == 4 else T - 1
+    parts = kh
     bf = jnp.bfloat16
     dma = pltpu.SemaphoreType.DMA
     vmem = pl.BlockSpec(memory_space=pltpu.VMEM)
@@ -798,8 +844,11 @@
             jax.ShapeDtypeStruct((token_count, cols), bf),
         ),
         in_specs=[hbm] * 8 + [vmem] * 7,
-        out_specs=(vmem, vmem),
+        out_specs=(hbm, hbm),
         scratch_shapes=[
+            pltpu.VMEM((rows, out_cols), bf),
+            pltpu.VMEM((token_count, cols), bf),
+            dma((1 + out_cols // math.gcd(out_cols, 256),)),
             pltpu.VMEM(moe_input.shape, bf),
             pltpu.VMEM(query_input.shape, bf),
             pltpu.VMEM(key_input.shape, bf),
@@ -818,7 +867,7 @@
             pltpu.VMEM((T, n, capp, ffl), bf),
             pltpu.VMEM((n, capp, cols), bf),
             pltpu.VMEM((n, capp, cols), bf),
-            pltpu.VMEM((T, rows, aw), bf),
+            pltpu.VMEM((T, parts, rows, aw // parts), bf),
             pltpu.VMEM((rows, out_cols), jnp.float32),
             pltpu.VMEM(gate.shape, bf),
             pltpu.VMEM(up.shape, bf),
@@ -841,8 +890,8 @@
             dma((slots, nz)),
             dma((n,)),
             dma((n,)),
-            dma((slots, 1)),
-            dma((slots, 1)),
+            dma((slots, parts)),
+            dma((slots, parts)),
         ],
         compiler_params=pltpu.CompilerParams(
             collective_id=0, has_side_effects=True, vmem_limit_bytes=63 * 1024 * 1024

time: 126 us -> 112 us (0.89)
  the two profiles are of different devices: /device:TPU:0 before, /device:TPU:1 now
where the time goes in v2:
time: 112 us
  Pallas kernels  107 us (96%)
  local copies, waits for them, and re-layouts  3.12 us (3%)
    pallas_call x1, Pallas kernels, on_device(): pl.pallas_call(functools.partial(kernel, (n, T, head_width)), out_shape=(...  107 us
    unnamed x4, local copies, waits for them, and re-layouts  3.12 us

profile of v2, /device:TPU:1, one launch (start us, length us, event | category | flops | bytes accessed | tf_op | source)
XLA Modules:
  0.0 111.9 jit_solution(2234643183545174976)
XLA Ops:
  0.7 0.8 negate_select_fusion
  1.5 107.2 %shard_map.140 = (bf16[512,1024]{1,0:T(8,128)(2,1)}, bf16[256,1024]{1,0:T(8,128)(2,1)}) custom-call(bf16[256,4096]{1,0:T(8,128)(2,1)} %x_hbm.1, bf16[512,512]{1,0:T(8,128)(2,1)} %q_hbm.1, bf16[512,256]{1,0:T(8,128)(2,1)} %k_hbm.1, bf16[512,256]{1,0:T(8,128)(2,1)} %v_hbm.1, bf16[4096,256]{1,0:T(8,128)(2,1)} %bitcast.8, bf16[4096,256]{1,0:T(8,128)(2,1)} %bitcast.9, ...), custom_call_target="tpu_custom_call" | custom-call | tf_op jit(solution)/shard_map/pallas_call | solution.py:840
  108.8 0.0 copy-start
  108.8 2.3 %copy.17 = bf16[512,1024]{1,0:T(8,128)(2,1)} copy(bf16[512,1024]{1,0:T(8,128)(2,1)} %get-tuple-element.6) | data formatting | bytes 2097152
  111.1 0.0 copy-done
  111.1 0.8 copy.18
  (3 shorter events, 0.0 us)
Async XLA Ops:
  108.8 2.3 %copy-start = (bf16[256,1024]{1,0:T(8,128)(2,1)S(1)}, bf16[256,1024]{1,0:T(8,128)(2,1)}, u32[]{:S(2)}) copy-start(bf16[256,1024]{1,0:T(8,128)(2,1)} %get-tuple-element.7) | copy-start | bytes 1572868

commit v3 on v2

--- a/solution.py
+++ b/solution.py
@@ -785,6 +785,28 @@
     lax.fori_loop(0, out_cols // half, drain_out, 0)
 
 
+def hand_over(attn_in, moe_in, attn_out, moe_out, attn_buf, moe_buf, in_sem, out_sem):
+    pieces = []
+    for src, buf, dst in ((attn_in, attn_buf, attn_out), (moe_in, moe_buf, moe_out)):
+        size = math.gcd(src.shape[0], 128)
+        for r in range(0, src.shape[0], size):
+            at = pl.ds(r, size)
+            i = len(pieces)
+            pieces.append(
+                (
+                    pltpu.make_async_copy(src.at[at], buf.at[at], in_sem.at[i]),
+                    pltpu.make_async_copy(buf.at[at], dst.at[at], out_sem.at[i]),
+                )
+            )
+    for read, _ in pieces:
+        read.start()
+    for read, write in pieces:
+        read.wait()
+        write.start()
+    for _, write in pieces:
+        write.wait()
+
+
 def on_device(
     n,
     T,
@@ -837,7 +859,7 @@
     dma = pltpu.SemaphoreType.DMA
     vmem = pl.BlockSpec(memory_space=pltpu.VMEM)
     hbm = pl.BlockSpec(memory_space=pl.ANY)
-    return pl.pallas_call(
+    attn, moe = pl.pallas_call(
         functools.partial(kernel, (n, T, head_width)),
         out_shape=(
             jax.ShapeDtypeStruct((rows, out_cols), bf),
@@ -913,6 +935,23 @@
         routes.T,
         route_weight.T,
     )
+    count = rows // math.gcd(rows, 128) + token_count // math.gcd(token_count, 128)
+    return pl.pallas_call(
+        hand_over,
+        out_shape=(
+            jax.ShapeDtypeStruct(attn.shape, bf),
+            jax.ShapeDtypeStruct(moe.shape, bf),
+        ),
+        in_specs=[hbm] * 2,
+        out_specs=(hbm, hbm),
+        scratch_shapes=[
+            pltpu.VMEM(attn.shape, bf),
+            pltpu.VMEM(moe.shape, bf),
+            dma((count,)),
+            dma((count,)),
+        ],
+        compiler_params=pltpu.CompilerParams(vmem_limit_bytes=63 * 1024 * 1024),
+    )(attn, moe)
 
 
 def solution(mesh):

time: 112 us -> 111 us (level)
  local copies, waits for them, and re-layouts: 3.12 us -> 0 us
  Pallas kernels: 107 us -> 109 us
    unnamed x4 -> x0, local copies, waits for them, and re-layouts: 3.12 us -> none
    pallas_call x0 -> x1, Pallas kernels: none -> 2.19 us  [on_device(): pl.pallas_call(hand_over, out_shape=(jax.ShapeDtypeStruct(attn.shape, bf)...]
where the time goes in v3:
time: 111 us
  Pallas kernels  109 us (98%)
    pallas_call x1, Pallas kernels, on_device(): pl.pallas_call(functools.partial(kernel, (n, T, head_width)), out_shape=(...  107 us

profile of v3, /device:TPU:1, one launch (start us, length us, event | category | flops | bytes accessed | tf_op | source)
XLA Modules:
  0.0 111.1 jit_solution(17646614312766879529)
XLA Ops:
  0.7 0.8 negate_select_fusion
  1.5 107.2 %shard_map.140 = (bf16[512,1024]{1,0:T(8,128)(2,1)}, bf16[256,1024]{1,0:T(8,128)(2,1)}) custom-call(bf16[256,4096]{1,0:T(8,128)(2,1)} %x_hbm.1, bf16[512,512]{1,0:T(8,128)(2,1)} %q_hbm.1, bf16[512,256]{1,0:T(8,128)(2,1)} %k_hbm.1, bf16[512,256]{1,0:T(8,128)(2,1)} %v_hbm.1, bf16[4096,256]{1,0:T(8,128)(2,1)} %bitcast.8, bf16[4096,256]{1,0:T(8,128)(2,1)} %bitcast.9, ...), custom_call_target="tpu_custom_call" | custom-call | tf_op jit(solution)/shard_map/pallas_call | solution.py:862
  108.8 2.2 %shard_map.141 = (bf16[512,1024]{1,0:T(8,128)(2,1)}, bf16[256,1024]{1,0:T(8,128)(2,1)}) custom-call(bf16[512,1024]{1,0:T(8,128)(2,1)} %get-tuple-element.4.attn_in, bf16[256,1024]{1,0:T(8,128)(2,1)} %get-tuple-element.5.moe_in), custom_call_target="tpu_custom_call" | custom-call | tf_op jit(solution)/shard_map/pallas_call | solution.py:939
  (3 shorter events, 0.0 us)
